TPU v7x, 32 devices: a whole 2x2x4 slice. The times are simulated.
32 devices in a mesh: st: 16 (over z, y, x), tp: 2 (over core).
Axes of the slice: x: 2, y: 2, z: 4, core: 2. Of those that a mesh axis runs over, the one named last changes fastest.
Arguments:
- tokens: bfloat16 [4096, 2048], P('st'), may hold values from -6 to 6
- store: bfloat16 [64, 64, 2048], P('st'), may hold values from -6 to 6
- passage_ids: int32 [64, 4], P('st'), may hold values from 0 to 63, as said below
- w_query: bfloat16 [2048, 2048], P(None, 'tp'), may hold values from -0.125 to 0.125
- w_key: bfloat16 [2048, 512], P(None, 'tp'), may hold values from -0.125 to 0.125
- w_value: bfloat16 [2048, 512], P(None, 'tp'), may hold values from -0.125 to 0.125
- w_ret_query: bfloat16 [2048, 1024], P(None, 'tp'), may hold values from -0.125 to 0.125
- w_ret_key: bfloat16 [2048, 1024], P(None, 'tp'), may hold values from -0.125 to 0.125
- w_ret_value: bfloat16 [2048, 2048], P(None, 'tp'), may hold values from -0.125 to 0.125
- ret_rate: float32 [8], P('tp'), may hold values from 0.003 to 0.03
- ret_gain: float32 [2048], P('tp'), may hold values from 0.1 to 1.9
- gate_logit: float32 [2048], P('tp'), may hold values from -2 to 2
- out_grad: bfloat16 [4096, 2048], P('st', 'tp'), may hold values from -6 to 6
Outputs:
- grad_tokens: bfloat16 [4096, 2048], P(('st', 'tp'))
- grad_store: bfloat16 [64, 64, 2048], P(('st', 'tp'))
- grad_key_weight: float32 [2048, 512], P(None, 'tp')
Inputs may be any that keep to these rules, and one draw needn't show every extreme that they name: `passage_ids`: passage p lies on index p // 4 of st. The rows of one device name exactly 1 passage of every owner, so the 4 passages of a block differ.
All inputs are finite; a program needn't handle non-finite values.
Results may differ from a plain program's by a relative error of at most 0.012.
Values may be sent and summed in bfloat16 or wider, within the bound.
A program may use at most 192 MiB of HBM per device.

v0:
```python
import jax
import jax.numpy as jnp
from jax import lax
from jax.sharding import PartitionSpec as P

HEAD = 256
BLK = 64
KP = 4
MOST = 1


EPSILON = 1.0


def retention_grads(query_rows, key_rows, value_rows, rates, gains, cotangent):
    length = query_rows.shape[0]
    heads = rates.shape[0]
    queries = query_rows.reshape(length, heads, -1)
    keyset = key_rows.reshape(length, heads, -1)
    values = value_rows.reshape(length, heads, -1)
    positions = jnp.arange(length, dtype=jnp.float32)
    distance = positions[:, None] - positions[None, :]
    damping = jnp.where(
        distance >= 0.0, jnp.exp(-rates[:, None, None] * jnp.maximum(distance, 0.0)), 0.0
    ) * queries.shape[-1] ** (-0.5)
    raw = jnp.einsum("thd,shd->hts", queries, keyset, preferred_element_type=jnp.float32)
    weights = (raw * damping).astype(jnp.bfloat16)
    mixed = jnp.einsum("hts,she->the", weights, values, preferred_element_type=jnp.float32)
    inverse = lax.rsqrt(jnp.mean(mixed * mixed, axis=-1, keepdims=True) + EPSILON)
    scaled = cotangent.astype(jnp.float32).reshape(length, heads, -1) * gains.reshape(heads, -1)
    inner = jnp.mean(scaled * mixed, axis=-1, keepdims=True)
    grad_mixed = (inverse * scaled - inverse * inverse * inverse * mixed * inner).astype(
        jnp.bfloat16
    )
    grad_weights = (
        jnp.einsum("the,she->hts", grad_mixed, values, preferred_element_type=jnp.float32) * damping
    ).astype(jnp.bfloat16)
    grad_first = (
        jnp.einsum("hts,shd->thd", grad_weights, keyset, preferred_element_type=jnp.float32)
        .astype(jnp.bfloat16)
        .reshape(length, -1)
    )
    grad_second = (
        jnp.einsum("hts,thd->shd", grad_weights, queries, preferred_element_type=jnp.float32)
        .astype(jnp.bfloat16)
        .reshape(length, -1)
    )
    grad_third = (
        jnp.einsum("hts,the->she", weights, grad_mixed, preferred_element_type=jnp.float32)
        .astype(jnp.bfloat16)
        .reshape(length, -1)
    )
    return (grad_first, grad_second, grad_third)


def against_rows(left, weight):
    return lax.dot_general(
        left, weight, (((1,), (1,)), ((), ())), preferred_element_type=jnp.float32
    )


def across_rows(left, right):
    return lax.dot_general(
        left, right, (((0,), (0,)), ((), ())), preferred_element_type=jnp.float32
    )


def per_device(
    tokens,
    store,
    passage_ids,
    w_query,
    w_key,
    w_value,
    w_ret_query,
    w_ret_key,
    w_ret_value,
    ret_rate,
    ret_gain,
    gate_logit,
    out_grad,
):
    owners = lax.axis_size("st")
    pass_dev, plen, width = store.shape
    length = tokens.shape[0]
    kv_width = w_key.shape[1]
    kv_local = kv_width // HEAD
    group = w_query.shape[1] // HEAD // kv_local
    blocks = length // BLK
    slot_ids = passage_ids.reshape(-1)
    slot_count = slot_ids.shape[0]
    slot_owner = slot_ids // pass_dev
    slot_local = slot_ids % pass_dev
    order = jnp.arange(slot_count, dtype=jnp.int32)
    same_owner = slot_owner[:, None] == slot_owner[None, :]
    rank = jnp.sum(same_owner & (order[None, :] < order[:, None]), axis=1)
    position = slot_owner * MOST + rank
    cells = owners * MOST
    placed = jnp.arange(cells, dtype=jnp.int32)[:, None] == position[None, :]
    request = (jnp.sum(jnp.where(placed, slot_local[None, :] + 1, 0), axis=1) - 1).reshape(
        owners, MOST
    )
    incoming = lax.all_to_all(request, "st", split_axis=0, concat_axis=0, tiled=True)
    wanted = incoming.reshape(-1)
    valid = wanted >= 0
    safe = jnp.maximum(wanted, 0)
    placed_bf = placed.astype(jnp.bfloat16)
    store_rows = store.reshape(-1, width)
    nothing = jnp.zeros((), jnp.bfloat16)
    own_kv = jnp.concatenate(
        [
            jnp.dot(store_rows, w_key, preferred_element_type=jnp.float32).astype(jnp.bfloat16),
            jnp.dot(store_rows, w_value, preferred_element_type=jnp.float32).astype(jnp.bfloat16),
        ],
        axis=1,
    ).reshape(pass_dev, plen, 2 * kv_width)
    reply = jnp.where(valid[:, None, None], own_kv[safe], nothing).reshape(
        owners, MOST, plen, 2 * kv_width
    )
    arrived = lax.all_to_all(reply, "st", split_axis=0, concat_axis=0, tiled=True)
    slot_kv = (
        across_rows(placed_bf, arrived.reshape(cells, -1))
        .astype(jnp.bfloat16)
        .reshape(slot_count, plen, 2 * kv_width)
    )
    factor = HEAD ** (-0.5)
    gate = jax.nn.sigmoid(gate_logit)
    query_bf = jnp.dot(tokens, w_query, preferred_element_type=jnp.float32).astype(jnp.bfloat16)
    queries = query_bf.reshape(blocks, BLK, kv_local, group, HEAD)
    keys = slot_kv[:, :, :kv_width].reshape(blocks, KP * plen, kv_local, HEAD)
    values = slot_kv[:, :, kv_width:].reshape(blocks, KP * plen, kv_local, HEAD)
    scores = (
        jnp.einsum("btkgd,bskd->bkgts", queries, keys, preferred_element_type=jnp.float32) * factor
    )
    expo = jnp.exp(scores)
    probs = expo / jnp.sum(expo, axis=-1, keepdims=True)
    probs_bf = probs.astype(jnp.bfloat16)
    attn = jnp.einsum("bkgts,bskd->btkgd", probs_bf, values, preferred_element_type=jnp.float32)
    grad_attn = out_grad.astype(jnp.float32).reshape(
        blocks, BLK, kv_local, group, HEAD
    ) * gate.reshape(kv_local, group, HEAD)
    grad_attn_bf = grad_attn.astype(jnp.bfloat16)
    grad_probs = jnp.einsum(
        "btkgd,bskd->bkgts", grad_attn_bf, values, preferred_element_type=jnp.float32
    )
    delta = jnp.moveaxis(jnp.sum(grad_attn * attn, axis=-1), 1, 3)
    grad_scores = (probs * (grad_probs - delta[..., None]) * factor).astype(jnp.bfloat16)
    grad_query = (
        jnp.einsum("bkgts,bskd->btkgd", grad_scores, keys, preferred_element_type=jnp.float32)
        .astype(jnp.bfloat16)
        .reshape(length, -1)
    )
    grad_keys = (
        jnp.einsum("bkgts,btkgd->bskd", grad_scores, queries, preferred_element_type=jnp.float32)
        .astype(jnp.bfloat16)
        .reshape(slot_count, plen, kv_width)
    )
    grad_values = (
        jnp.einsum("bkgts,btkgd->bskd", probs_bf, grad_attn_bf, preferred_element_type=jnp.float32)
        .astype(jnp.bfloat16)
        .reshape(slot_count, plen, kv_width)
    )
    slot_grad = jnp.concatenate([grad_keys, grad_values], axis=2)
    outgoing = (
        jnp.dot(placed_bf, slot_grad.reshape(slot_count, -1), preferred_element_type=jnp.float32)
        .astype(jnp.bfloat16)
        .reshape(owners, MOST, plen, 2 * kv_width)
    )
    returned = lax.all_to_all(outgoing, "st", split_axis=0, concat_axis=0, tiled=True)
    matched = (jnp.arange(pass_dev, dtype=jnp.int32)[:, None] == wanted[None, :]).astype(
        jnp.bfloat16
    )
    passage_grad = jnp.dot(
        matched, returned.reshape(cells, -1), preferred_element_type=jnp.float32
    ).reshape(pass_dev * plen, 2 * kv_width)
    key_grad = passage_grad[:, :kv_width]
    upper = key_grad.astype(jnp.bfloat16)
    lower = (key_grad - upper.astype(jnp.float32)).astype(jnp.bfloat16)
    key_term = across_rows(store_rows, upper) + across_rows(store_rows, lower)
    grad_key_weight = lax.psum(key_term, "st")
    passage_bf = passage_grad.astype(jnp.bfloat16)
    grad_store = lax.psum_scatter(
        (
            against_rows(passage_bf[:, :kv_width], w_key)
            + against_rows(passage_bf[:, kv_width:], w_value)
        ).astype(jnp.bfloat16),
        "tp",
        scatter_dimension=0,
        tiled=True,
    ).astype(jnp.float32)
    grad_store = grad_store.astype(jnp.bfloat16).reshape(-1, plen, width)
    ret_query = jnp.dot(tokens, w_ret_query, preferred_element_type=jnp.float32).astype(
        jnp.bfloat16
    )
    ret_key = jnp.dot(tokens, w_ret_key, preferred_element_type=jnp.float32).astype(jnp.bfloat16)
    ret_value = jnp.dot(tokens, w_ret_value, preferred_element_type=jnp.float32).astype(
        jnp.bfloat16
    )
    grad_rq, grad_rk, grad_rv = retention_grads(
        ret_query, ret_key, ret_value, ret_rate, ret_gain, out_grad
    )
    total = against_rows(grad_query, w_query)
    total = total + against_rows(grad_rq, w_ret_query)
    total = total + against_rows(grad_rk, w_ret_key)
    grad_tokens = lax.psum_scatter(
        (total + against_rows(grad_rv, w_ret_value)).astype(jnp.bfloat16),
        "tp",
        scatter_dimension=0,
        tiled=True,
    )
    return (grad_tokens, grad_store, grad_key_weight)


def solution(mesh):
    return jax.shard_map(
        per_device,
        mesh=mesh,
        in_specs=(
            P("st", None),
            P("st", None, None),
            P("st", None),
            P(None, "tp"),
            P(None, "tp"),
            P(None, "tp"),
            P(None, "tp"),
            P(None, "tp"),
            P(None, "tp"),
            P("tp"),
            P("tp"),
            P("tp"),
            P("st", "tp"),
        ),
        out_specs=(P(("st", "tp"), None), P(("st", "tp"), None, None), P(None, "tp")),
        check_vma=False,
    )
```

profile of v0, /device:TPU:0, one launch (start us, length us, event | category | flops | bytes accessed | tf_op | source)
XLA Modules:
  0.0 243.0 jit_solution(17686899952723807470)
XLA Ops:
  8.0 0.9 reshape.304
  9.3 0.7 copy.79
  10.0 8.3 %all-to-all-start = ((s32[16,1,1]{2,1,0:T(1,128)}), s32[16,1,1]{2,1,0:T(1,128)S(1)}, u32[]{:S(2)}, u32[]{:S(2)}) async-start(s32[16,1,1]{2,1,0:T(1,128)} %copy.79), calls=%async_computation | async-start | bytes 16384 | tf_op jit(solution)/shard_map/all_to_all | solution.py:103
  18.3 2.1 convolution_convert_fusion.10
  20.5 0.5 convolution_convert_fusion.11
  21.1 0.7 pad_maximum_fusion.1
  21.8 1.1 copy.80
  22.9 2.7 %all-to-all-done = s32[16,1,1]{2,1,0:T(1,128)S(1)} async-done(((s32[16,1,1]{2,1,0:T(1,128)}), s32[16,1,1]{2,1,0:T(1,128)S(1)}, u32[]{:S(2)}, u32[]{:S(2)}) %all-to-all-start) | async-done | bytes 96 | tf_op jit(solution)/shard_map/all_to_all | solution.py:103
  25.5 0.7 fusion.45
  26.2 1.6 gather_fusion
  27.8 0.4 compare_reduce_fusion
  28.2 2.4 fusion.18
  30.6 4.3 %all-to-all-start.1 = ((bf16[16,1,64,512]{3,2,1,0:T(8,128)(2,1)}), bf16[16,1,64,512]{3,2,1,0:T(8,128)(2,1)}, u32[]{:S(2)}, u32[]{:S(2)}) async-start(bf16[16,1,64,512]{3,2,1,0:T(8,128)(2,1)} %fusion.18), calls=%async_computation.1 | async-start | bytes 2097152 | tf_op jit(solution)/shard_map/all_to_all | solution.py:120
  34.9 2.2 copy.89
  37.2 2.5 %reshape.312 = f32[4,64,4,256]{3,2,1,0:T(4,128)} reshape(bf16[256,1024]{1,0:T(8,128)(2,1)} %param.25) | data formatting | bytes 1572864 | tf_op jit(solution)/shard_map/reshape | solution.py:139
  39.7 2.5 %reshape.313 = f32[4,64,1,4,256]{4,3,1,0,2:T(4,128)} reshape(bf16[256,1024]{1,0:T(8,128)(2,1)} %param.25) | data formatting | bytes 1572864 | tf_op jit(solution)/shard_map/reshape | solution.py:139
  42.2 1.9 convolution_convert_fusion.8
  44.2 0.8 copy.103
  45.0 3.3 %convolution_convert_fusion.9 = bf16[256,512]{1,0:T(8,128)(2,1)} fusion(bf16[256,2048]{1,0:T(8,128)(2,1)} %param.13, bf16[2048,512]{1,0:T(8,128)(2,1)} %param.20), kind=kOutput, calls=%fused_computation.40 | convolution fusion | flops 537001984 | bytes 3407872 | tf_op jit(solution)/shard_map/dot_general | solution.py:195
  48.3 1.1 copy.102
  49.4 4.6 %convolution_convert_fusion.5 = bf16[256,1024]{1,0:T(8,128)(2,1)} fusion(bf16[256,2048]{1,0:T(8,128)(2,1)} %param.13, bf16[2048,1024]{1,0:T(8,128)(2,1)} %param.16), kind=kOutput, calls=%fused_computation.33 | convolution fusion | flops 1074003968 | bytes 5767168 | tf_op jit(solution)/shard_map/dot_general | solution.py:128
  54.0 2.2 reshape.310
  56.3 0.8 fusion.29
  57.0 1.7 all-to-all-done.1
  58.7 1.8 copy.105
  60.5 0.5 convolution_convert_fusion.1
  61.0 0.3 copy.106
  61.4 0.8 copy-done.4
  62.2 0.4 fusion.47
  62.8 0.6 fusion.14
  63.4 0.6 copy-done.19
  64.0 0.5 fusion.15
  64.5 0.4 fusion.16
  64.9 0.4 fusion.13
  65.3 0.4 copy-done.10
  65.8 0.6 copy.108
  66.4 0.4 convolution_convert_fusion
  66.8 1.3 copy.109
  68.2 6.0 %all-to-all-start.2 = ((bf16[16,1,64,512]{3,2,1,0:T(8,128)(2,1)}), bf16[16,1,64,512]{3,2,1,0:T(8,128)(2,1)}, u32[]{:S(2)}, u32[]{:S(2)}) async-start(bf16[16,1,64,512]{3,2,1,0:T(8,128)(2,1)} %bitcast.183), calls=%async_computation.3 | async-start | bytes 2097152 | tf_op jit(solution)/shard_map/all_to_all | solution.py:169
  74.4 1.5 fusion.10
  75.9 4.0 %convolution_convert_fusion.4 = bf16[256,1024]{1,0:T(8,128)(2,1)S(1)} fusion(bf16[256,2048]{1,0:T(8,128)(2,1)} %param.13, bf16[2048,1024]{1,0:T(8,128)(2,1)} %param.21), kind=kOutput, calls=%fused_computation.32 | convolution fusion | flops 1074003968 | bytes 5767168 | tf_op jit(solution)/shard_map/dot_general | solution.py:196
  79.9 0.4 multiply_reduce_fusion.1
  80.6 0.8 copy-done.12
  81.4 0.5 fusion.12
  81.9 0.8 copy-done.16
  82.7 0.9 convolution_convert_fusion.6
  83.6 13.5 %all-to-all-done.2 = bf16[16,1,64,512]{3,2,1,0:T(8,128)(2,1)} async-done(((bf16[16,1,64,512]{3,2,1,0:T(8,128)(2,1)}), bf16[16,1,64,512]{3,2,1,0:T(8,128)(2,1)}, u32[]{:S(2)}, u32[]{:S(2)}) %all-to-all-start.2) | async-done | bytes 1048608 | tf_op jit(solution)/shard_map/all_to_all | solution.py:169
  97.2 1.8 copy.110
  99.0 1.1 fusion.40
  100.1 2.2 reshape.329
  102.3 1.5 fusion.36
  103.8 1.8 fusion.1
  105.6 1.4 convolution_convert_fusion.7
  107.4 3.7 %fusion.49 = f32[256,2048]{1,0:T(8,128)S(1)} fusion(bf16[256,1024]{0,1:T(8,128)(2,1)S(1)} %bitcast.195, bf16[2048,1024]{1,0:T(8,128)(2,1)} %param.21), kind=kOutput, calls=%fused_computation.101 | convolution fusion | flops 1073741824 | bytes 6815744 | tf_op jit(solution)/shard_map/dot_general | solution.py:57
  111.1 0.3 fusion.17
  111.4 0.4 copy.85
  111.9 1.3 fusion.48
  113.3 0.8 convolution_add_fusion.1
  114.1 0.8 copy-done.17
  114.8 1.7 fusion.2
  116.7 1.8 fusion.34
  118.5 1.5 fusion.3
  120.0 112.7 %all-reduce.2.cloned.1.call-done = f32[2048,256]{0,1:T(8,128)} async-done(((f32[2048,256]{0,1:T(8,128)}), f32[2048,256]{0,1:T(8,128)}) %all-reduce.2.cloned.1.call-update) | async-done | bytes 2097168 | tf_op jit(solution)/shard_map/psum | solution.py:180
  232.7 2.9 %copy.96 = f32[2048,256]{1,0:T(8,128)} copy(f32[2048,256]{0,1:T(8,128)} %all-reduce.2.cloned.1.call-done) | data formatting | bytes 4194304
  (74 shorter events, 1.9 us)
Async XLA Ops:
  8.0 34.2 %copy-start = (bf16[2048,512]{1,0:T(8,128)(2,1)S(1)}, bf16[2048,512]{1,0:T(8,128)(2,1)}, u32[]{:S(2)}) copy-start(bf16[2048,512]{1,0:T(8,128)(2,1)} %param.19) | copy-start | bytes 6291460
  8.0 12.5 %copy-start.1 = (bf16[4,64,2048]{2,1,0:T(8,128)(2,1)S(1)}, bf16[4,64,2048]{2,1,0:T(8,128)(2,1)}, u32[]{:S(2)}) copy-start(bf16[4,64,2048]{2,1,0:T(8,128)(2,1)} %param.14) | copy-start | bytes 3145732
  10.0 15.6 %all-to-all-start = ((s32[16,1,1]{2,1,0:T(1,128)}), s32[16,1,1]{2,1,0:T(1,128)S(1)}, u32[]{:S(2)}, u32[]{:S(2)}) async-start(s32[16,1,1]{2,1,0:T(1,128)} %copy.79), calls=%async_computation | async-start | bytes 16384 | tf_op jit(solution)/shard_map/all_to_all | solution.py:103
  18.3 2.2 copy-start.8
  30.6 28.1 %all-to-all-start.1 = ((bf16[16,1,64,512]{3,2,1,0:T(8,128)(2,1)}), bf16[16,1,64,512]{3,2,1,0:T(8,128)(2,1)}, u32[]{:S(2)}, u32[]{:S(2)}) async-start(bf16[16,1,64,512]{3,2,1,0:T(8,128)(2,1)} %fusion.18), calls=%async_computation.1 | async-start | bytes 2097152 | tf_op jit(solution)/shard_map/all_to_all | solution.py:120
  34.9 7.3 %copy-start.26 = (f32[4]{0:T(128)S(1)}, f32[4]{0:T(128)}, u32[]{:S(2)}) copy-start(f32[4]{0:T(128)} %param.22) | copy-start | bytes 52
  34.9 7.2 %copy-start.23 = (f32[1024]{0:T(1024)S(1)}, f32[1024]{0:T(1024)}, u32[]{:S(2)}) copy-start(f32[1024]{0:T(1024)} %param.23) | copy-start | bytes 12292
  34.9 7.2 %copy-start.24 = (f32[1024]{0:T(1024)S(1)}, f32[1024]{0:T(1024)}, u32[]{:S(2)}) copy-start(f32[1024]{0:T(1024)} %param.24) | copy-start | bytes 12292
  61.0 1.2 copy-start.3
  61.3 1.5 copy-start.18
  61.4 0.8 copy-start.4
  62.8 1.2 copy-start.19
  64.9 0.8 copy-start.10
  68.2 29.0 %all-to-all-start.2 = ((bf16[16,1,64,512]{3,2,1,0:T(8,128)(2,1)}), bf16[16,1,64,512]{3,2,1,0:T(8,128)(2,1)}, u32[]{:S(2)}, u32[]{:S(2)}) async-start(bf16[16,1,64,512]{3,2,1,0:T(8,128)(2,1)} %bitcast.183), calls=%async_computation.3 | async-start | bytes 2097152 | tf_op jit(solution)/shard_map/all_to_all | solution.py:169
  74.1 158.6 %all-reduce.2.cloned.1.call-start = ((), (), s32[]{:S(2)}) async-start(), calls=%async_computation.7 | async-start | bytes 4194304 | tf_op jit(solution)/shard_map/psum | solution.py:180
  75.9 4.0 %copy-start.14 = (bf16[4,256,256]{2,1,0:T(8,128)(2,1)}, bf16[4,256,256]{2,1,0:T(8,128)(2,1)S(1)}, u32[]{:S(2)}) copy-start(bf16[4,256,256]{2,1,0:T(8,128)(2,1)S(1)} %fusion.10) | copy-start | bytes 1572868
  75.9 4.0 %copy-start.2 = (f32[256,1024]{0,1:T(8,128)S(1)}, f32[256,1024]{0,1:T(8,128)}, u32[]{:S(2)}) copy-start(f32[256,1024]{0,1:T(8,128)} %copy.89) | copy-start | bytes 3145732
  80.3 1.1 copy-start.22
  80.6 0.8 copy-start.12
  81.4 1.3 copy-start.20
  81.9 0.8 copy-start.16
  102.3 1.5 copy-start.6
  105.5 1.5 copy-start.13
  105.5 1.5 copy-start.15
  105.6 130.0 %reduce-scatter.3.cloned.1.call-start = ((), (), s32[]{:S(2)}) async-start(), calls=%async_computation.5 | async-start | bytes 1572864 | tf_op jit(solution)/shard_map/reduce_scatter | solution.py:205
  107.4 3.7 %copy-start.5 = (bf16[16,64,256]{2,1,0:T(8,128)(2,1)S(1)}, bf16[16,64,256]{2,1,0:T(8,128)(2,1)}, u32[]{:S(2)}) copy-start(bf16[16,64,256]{2,1,0:T(8,128)(2,1)} %copy-done.4) | copy-start | bytes 1572868
  107.4 3.7 %copy-start.11 = (bf16[4,4,64,256]{3,2,1,0:T(8,128)(2,1)S(1)}, bf16[4,4,64,256]{3,2,1,0:T(8,128)(2,1)}, u32[]{:S(2)}) copy-start(bf16[4,4,64,256]{3,2,1,0:T(8,128)(2,1)} %copy-done.10) | copy-start | bytes 1572868
  107.4 4.5 %copy-start.25 = (bf16[2048,1024]{1,0:T(8,128)(2,1)S(1)}, bf16[2048,1024]{1,0:T(8,128)(2,1)}, u32[]{:S(2)}) copy-start(bf16[2048,1024]{1,0:T(8,128)(2,1)} %param.16) | copy-start | bytes 12582916
  113.2 1.6 copy-start.17
  113.3 1.6 copy-start.21
  114.8 1.8 copy-start.7
  116.6 119.0 %reduce-scatter.5.cloned.1.call-start = ((), (), s32[]{:S(2)}) async-start(), calls=%async_computation.6 | async-start | bytes 1572864 | tf_op jit(solution)/shard_map/reduce_scatter | solution.py:182
  116.7 1.8 copy-start.9
Sparse Core Ops, SparseCore 0:
  105.7 126.9 all-reduce.1
Sparse Core Ops, SparseCore 1:
  116.7 8.7 reduce-scatter.2
  128.1 9.5 reduce-scatter.4
where the time goes:
time: 244 us; the launch traced here: 243 us
  waiting for transfers between devices  131 us (54%)
  matrix products  40.1 us (16%)
  local copies, waits for them, and re-layouts  31.6 us (13%)
  starting transfers between devices  19 us (8%)
  between operations  16 us (7%)
  other arithmetic  5.71 us (2%)
    psum x1, waiting for transfers between devices, per_device(): grad_key_weight = lax.psum(key_term, 'st')  113 us
    all_to_all x1, waiting for transfers between devices, per_device(): lax.all_to_all(outgoing, 'st', split_axis=0, concat_axis=0, tiled=True)  13.5 us
    unnamed x61, local copies, waits for them, and re-layouts  13.2 us
    dot_general x6, matrix products, against_rows(): lax.dot_general(left, weight, (((1,), (1,)), ((), ())), preferred_element...  10.7 us
    all_to_all x1, starting transfers between devices, per_device(): lax.all_to_all(request, 'st', split_axis=0, concat_axis=0, tiled=True)  8.34 us
    all_to_all x1, starting transfers between devices, per_device(): lax.all_to_all(outgoing, 'st', split_axis=0, concat_axis=0, tiled=True)  5.96 us
    reshape x2, local copies, waits for them, and re-layouts, per_device(): out_grad.astype(jnp.float32).reshape(blocks, BLK, kv_local, group, HEAD)  4.98 us
  transfers between devices with their start and end apart: 6, of which 4 were waited for; matrix products, arithmetic and copies ran while one was open for 21% of the time, Pallas kernels for 0%

commit v1 on v0

--- a/solution.py
+++ b/solution.py
@@ -1,6 +1,10 @@
+import functools
+
 import jax
 import jax.numpy as jnp
 from jax import lax
+from jax.experimental import pallas as pl
+from jax.experimental.pallas import tpu as pltpu
 from jax.sharding import PartitionSpec as P
 
 HEAD = 256
@@ -65,7 +69,7 @@
     )
 
 
-def per_device(
+def per_device_plain(
     tokens,
     store,
     passage_ids,
@@ -211,9 +215,615 @@
     return (grad_tokens, grad_store, grad_key_weight)
 
 
+PLANE = 4
+HALVES = 2
+TILE = 256
+BF = jnp.bfloat16
+F32 = jnp.float32
+MESH = pl.DeviceIdType.MESH
+
+
+def nn(a, b):
+    return lax.dot_general(a, b, (((1,), (0,)), ((), ())), preferred_element_type=F32)
+
+
+def nt(a, b):
+    return lax.dot_general(a, b, (((1,), (1,)), ((), ())), preferred_element_type=F32)
+
+
+def tn(a, b):
+    return lax.dot_general(a, b, (((0,), (0,)), ((), ())), preferred_element_type=F32)
+
+
+def fused_kernel(
+    n,
+    ids_ref,
+    rate_ref,
+    gain_ref,
+    gate_ref,
+    tokens_hbm,
+    store_hbm,
+    wq_hbm,
+    wk_hbm,
+    wv_hbm,
+    wrq_hbm,
+    wrk_hbm,
+    wrv_hbm,
+    og_hbm,
+    gt_hbm,
+    gs_hbm,
+    gkw_hbm,
+    tokens,
+    store,
+    wq,
+    wk,
+    wv,
+    wrq,
+    wrk,
+    wrv,
+    og,
+    q,
+    rq,
+    rk,
+    rv,
+    gq,
+    grq,
+    grk,
+    grv,
+    total,
+    gt,
+    gt_in,
+    gs,
+    gs_in,
+    own_kv,
+    req_out,
+    req_in,
+    kv_out,
+    kv_in,
+    stage_k,
+    stage_v,
+    gk_out,
+    gv_out,
+    gk_in,
+    gv_in,
+    pk,
+    pv,
+    kt,
+    p1_in,
+    p1_sum,
+    p2_in,
+    kg,
+    owner_of,
+    slot_of,
+    load_sem,
+    out_sem,
+    tp_send,
+    tp_recv,
+    req_send,
+    req_recv,
+    kv_send,
+    kv_recv,
+    gk_send,
+    gk_recv,
+    gv_send,
+    gv_recv,
+    p1_send,
+    p1_recv,
+    p2_send,
+    p2_recv,
+    p3_send,
+    p3_recv,
+    p4_send,
+    p4_recv,
+):
+    me = lax.axis_index("st")
+    tp = lax.axis_index("tp")
+    length = tokens.shape[0]
+    width = tokens.shape[1]
+    plen = kv_in.shape[1]
+    pass_dev = store.shape[0] // plen
+    blocks = length // BLK
+    slots = blocks * KP
+    group = q.shape[1] // HEAD
+    ret_heads = rate_ref.shape[0]
+    depth = n // PLANE
+    my_q = lax.rem(me, PLANE)
+    my_z = lax.div(me, PLANE)
+    half_tok = length // 2
+    half_store = store.shape[0] // 2
+
+    pairs = (
+        (store_hbm, store),
+        (wk_hbm, wk),
+        (wv_hbm, wv),
+        (tokens_hbm, tokens),
+        (wrq_hbm, wrq),
+        (wrk_hbm, wrk),
+        (wrv_hbm, wrv),
+        (og_hbm, og),
+        (wq_hbm, wq),
+    )
+    loads = [pltpu.make_async_copy(a, b, load_sem.at[i]) for i, (a, b) in enumerate(pairs)]
+    for load in loads:
+        load.start()
+
+    barrier = pltpu.get_barrier_semaphore()
+
+    def greet(i, carry):
+        pl.semaphore_signal(
+            barrier, inc=1, device_id={"st": lax.rem(me + i, n)}, device_id_type=MESH
+        )
+        return carry
+
+    lax.fori_loop(1, n, greet, 0)
+    pl.semaphore_signal(barrier, inc=1, device_id={"tp": 1 - tp}, device_id_type=MESH)
+
+    for s in range(slots):
+        owner_of[s] = lax.div(ids_ref[s // KP, s % KP], pass_dev)
+
+    def invert(o, carry):
+        local = jnp.int32(0)
+        where = jnp.int32(0)
+        for s in range(slots):
+            ident = ids_ref[s // KP, s % KP]
+            hit = owner_of[s] == o
+            local = jnp.where(hit, lax.rem(ident, pass_dev), local)
+            where = jnp.where(hit, jnp.int32(s), where)
+        slot_of[o] = where
+        req_out[o] = jnp.full(req_out.shape[1:], local, jnp.int32)
+        return carry
+
+    lax.fori_loop(0, n, invert, 0)
+
+    def exchange(out_ref, in_ref, send, recv, i):
+        target = lax.rem(me + i, n)
+        return pltpu.make_async_remote_copy(
+            src_ref=out_ref.at[target],
+            dst_ref=in_ref.at[me],
+            send_sem=send.at[target],
+            recv_sem=recv.at[me],
+            device_id={"st": target},
+            device_id_type=MESH,
+        )
+
+    def arrival(out_ref, in_ref, send, recv, i):
+        source = lax.rem(me + i, n)
+        return pltpu.make_async_remote_copy(
+            src_ref=out_ref.at[source],
+            dst_ref=in_ref.at[source],
+            send_sem=send.at[source],
+            recv_sem=recv.at[source],
+            device_id={"st": source},
+            device_id_type=MESH,
+        )
+
+    def start_all(*refs):
+        def body(i, carry):
+            exchange(*refs, i).start()
+            return carry
+
+        lax.fori_loop(1, n, body, 0)
+
+    def wait_recv_all(*refs):
+        def body(i, carry):
+            arrival(*refs, i).wait_recv()
+            return carry
+
+        lax.fori_loop(1, n, body, 0)
+
+    def wait_send_all(*refs):
+        def body(i, carry):
+            exchange(*refs, i).wait_send()
+            return carry
+
+        lax.fori_loop(1, n, body, 0)
+
+    reqs = (req_out, req_in, req_send, req_recv)
+    kvs = (kv_out, kv_in, kv_send, kv_recv)
+    gks = (gk_out, gk_in, gk_send, gk_recv)
+    gvs = (gv_out, gv_in, gv_send, gv_recv)
+
+    pl.semaphore_wait(barrier, n)
+    start_all(*reqs)
+    req_in[me] = req_out[me]
+
+    for load in loads[:3]:
+        load.wait()
+    own_kv[:, :HEAD] = nn(store[...], wk[...]).astype(BF)
+    own_kv[:, HEAD:] = nn(store[...], wv[...]).astype(BF)
+    wait_recv_all(*reqs)
+
+    def names(r, p, lanes):
+        row = jnp.where(req_in[r][0:1, :] == p, 1.0, 0.0).astype(F32)
+        return jnp.concatenate([row] * (lanes // row.shape[1]), axis=1)
+
+    def select(r, carry):
+        chosen = jnp.zeros((plen, 2 * HEAD), F32)
+        for p in range(pass_dev):
+            chosen = chosen + names(r, p, 2 * HEAD) * own_kv[p * plen : (p + 1) * plen, :].astype(F32)
+        kv_out[r] = chosen.astype(BF)
+        return carry
+
+    lax.fori_loop(0, n, select, 0)
+    kv_in[me] = kv_out[me]
+    start_all(*kvs)
+
+    def project(w, out):
+        def body(i, carry):
+            cols = pl.ds(pl.multiple_of(i * TILE, TILE), TILE)
+            out[:, cols] = nn(tokens[...], w[:, cols]).astype(BF)
+            return carry
+
+        lax.fori_loop(0, w.shape[1] // TILE, body, 0)
+
+    loads[3].wait()
+    for load, w, out in ((loads[4], wrq, rq), (loads[5], wrk, rk), (loads[6], wrv, rv)):
+        load.wait()
+        project(w, out)
+    loads[7].wait()
+
+    ret_key = rq.shape[1] // ret_heads
+    ret_value = rv.shape[1] // ret_heads
+    at_t = lax.broadcasted_iota(jnp.int32, (length, length), 0)
+    at_s = lax.broadcasted_iota(jnp.int32, (length, length), 1)
+    distance = (at_t - at_s).astype(F32)
+
+    def retention(j, carry):
+        kc = pl.ds(pl.multiple_of(j * ret_key, ret_key), ret_key)
+        vc = pl.ds(pl.multiple_of(j * ret_value, ret_value), ret_value)
+        damping = jnp.where(
+            distance >= 0.0, jnp.exp(-rate_ref[j] * jnp.maximum(distance, 0.0)), 0.0
+        ) * ret_key ** (-0.5)
+        weights = (nt(rq[:, kc], rk[:, kc]) * damping).astype(BF)
+        y = nn(weights, rv[:, vc])
+        r = lax.rsqrt(jnp.mean(y * y, axis=1, keepdims=True) + EPSILON)
+        c = og[:, vc].astype(F32) * gain_ref[:, vc]
+        inner = jnp.mean(c * y, axis=1, keepdims=True)
+        gy = (r * c - r * r * r * y * inner).astype(BF)
+        gw = (nt(gy, rv[:, vc]) * damping).astype(BF)
+        grq[:, kc] = nn(gw, rk[:, kc]).astype(BF)
+        grk[:, kc] = tn(gw, rq[:, kc]).astype(BF)
+        grv[:, vc] = tn(weights, gy).astype(BF)
+        return carry
+
+    lax.fori_loop(0, ret_heads, retention, 0)
+    loads[8].wait()
+    project(wq, q)
+
+    def ret_total(i, carry):
+        rows = pl.ds(pl.multiple_of(i * TILE, TILE), TILE)
+        total[:, rows] = (
+            nt(grq[...], wrq[rows, :]) + nt(grk[...], wrk[rows, :]) + nt(grv[...], wrv[rows, :])
+        )
+        return carry
+
+    lax.fori_loop(0, width // TILE, ret_total, 0)
+
+    wait_recv_all(*kvs)
+    factor = HEAD ** (-0.5)
+
+    def attend(b, carry):
+        rows = pl.ds(pl.multiple_of(b * BLK, BLK), BLK)
+        read = [kv_in[owner_of[b * KP + k]] for k in range(KP)]
+        keys = jnp.concatenate([x[:, :HEAD] for x in read], axis=0)
+        values = jnp.concatenate([x[:, HEAD:] for x in read], axis=0)
+        cols = [slice(g * HEAD, (g + 1) * HEAD) for g in range(group)]
+        queries = jnp.concatenate([q[rows, c] for c in cols], axis=0)
+        expo = jnp.exp(nt(queries, keys) * factor)
+        probs = expo / jnp.sum(expo, axis=1, keepdims=True)
+        probs_bf = probs.astype(BF)
+        attn = nn(probs_bf, values)
+        grad_attn = jnp.concatenate(
+            [
+                og[rows, c].astype(F32) * (1.0 / (1.0 + jnp.exp(-gate_ref[:, c])))
+                for c in cols
+            ],
+            axis=0,
+        )
+        grad_attn_bf = grad_attn.astype(BF)
+        grad_probs = nt(grad_attn_bf, values)
+        delta = jnp.sum(grad_attn * attn, axis=1, keepdims=True)
+        scores = (probs * (grad_probs - delta) * factor).astype(BF)
+        grad_query = nn(scores, keys).astype(BF)
+        for g, c in enumerate(cols):
+            gq[rows, c] = grad_query[g * BLK : (g + 1) * BLK, :]
+        dk = tn(scores, queries).astype(BF)
+        dv = tn(probs_bf, grad_attn_bf).astype(BF)
+        for k in range(KP):
+            stage_k[b * KP + k] = dk[k * plen : (k + 1) * plen, :]
+            stage_v[b * KP + k] = dv[k * plen : (k + 1) * plen, :]
+        return carry
+
+    lax.fori_loop(0, blocks, attend, 0)
+
+    def place(stage, out):
+        def body(o, carry):
+            out[o] = stage[slot_of[o]]
+            return carry
+
+        lax.fori_loop(0, n, body, 0)
+
+    place(stage_k, gk_out)
+    place(stage_v, gv_out)
+    gk_in[me] = gk_out[me]
+    gv_in[me] = gv_out[me]
+    start_all(*gks)
+    start_all(*gvs)
+
+    def finish_total(i, carry):
+        rows = pl.ds(pl.multiple_of(i * TILE, TILE), TILE)
+        gt[:, rows] = (total[:, rows] + nt(gq[...], wq[rows, :])).astype(BF)
+        return carry
+
+    lax.fori_loop(0, width // TILE, finish_total, 0)
+
+    def to_partner(out_ref, in_ref, half, at):
+        return pltpu.make_async_remote_copy(
+            src_ref=out_ref.at[pl.ds(pl.multiple_of((1 - tp) * half, half), half)],
+            dst_ref=in_ref,
+            send_sem=tp_send.at[at],
+            recv_sem=tp_recv.at[at],
+            device_id={"tp": 1 - tp},
+            device_id_type=MESH,
+        )
+
+    def add_own(out_ref, in_ref, half):
+        own = out_ref[pl.ds(pl.multiple_of(tp * half, half), half), :]
+        in_ref[...] = (own.astype(F32) + in_ref[...].astype(F32)).astype(BF)
+
+    token_swap = to_partner(gt, gt_in, half_tok, 0)
+    token_swap.start()
+
+    def gather_sum(in_ref, out_ref):
+        for p in range(pass_dev):
+
+            def body(r, acc):
+                return acc + names(r, p, HEAD) * in_ref[r].astype(F32)
+
+            acc = lax.fori_loop(0, n, body, jnp.zeros((plen, HEAD), F32))
+            out_ref[p * plen : (p + 1) * plen, :] = acc.astype(BF)
+
+    wait_recv_all(*gks)
+    gather_sum(gk_in, pk)
+    piece = kt.shape[1]
+    per_tile = TILE // piece
+
+    def key_term(i, carry):
+        cols = pl.ds(pl.multiple_of(i * TILE, TILE), TILE)
+        term = tn(store[:, cols], pk[...]).astype(BF)
+        kt[pl.ds(i * per_tile, per_tile)] = term.reshape(per_tile, piece, HEAD)
+        return carry
+
+    lax.fori_loop(0, width // TILE, key_term, 0)
+
+    def chunk(h, quarter):
+        return pl.ds((h * PLANE + quarter) * depth, depth)
+
+    def plane_reduce(h, i):
+        other = lax.rem(my_q + i, PLANE)
+        return pltpu.make_async_remote_copy(
+            src_ref=kt.at[chunk(h, other)],
+            dst_ref=p1_in.at[h, i - 1],
+            send_sem=p1_send.at[h, i - 1],
+            recv_sem=p1_recv.at[h, i - 1],
+            device_id={"st": my_z * PLANE + other},
+            device_id_type=MESH,
+        )
+
+    def column_reduce(h, i):
+        other = lax.rem(my_z + i, depth)
+        return pltpu.make_async_remote_copy(
+            src_ref=p1_sum.at[h, other],
+            dst_ref=p2_in.at[h, i - 1],
+            send_sem=p2_send.at[h, i - 1],
+            recv_sem=p2_recv.at[h, i - 1],
+            device_id={"st": other * PLANE + my_q},
+            device_id_type=MESH,
+        )
+
+    def column_gather(h, i, source):
+        at = kg.at[(h * PLANE + my_q) * depth + source]
+        return pltpu.make_async_remote_copy(
+            src_ref=at,
+            dst_ref=at,
+            send_sem=p3_send.at[h, i - 1],
+            recv_sem=p3_recv.at[h, i - 1],
+            device_id={"st": lax.rem(my_z + i, depth) * PLANE + my_q},
+            device_id_type=MESH,
+        )
+
+    def plane_gather(h, i, source):
+        at = kg.at[chunk(h, source)]
+        return pltpu.make_async_remote_copy(
+            src_ref=at,
+            dst_ref=at,
+            send_sem=p4_send.at[h, i - 1],
+            recv_sem=p4_recv.at[h, i - 1],
+            device_id={"st": my_z * PLANE + lax.rem(my_q + i, PLANE)},
+            device_id_type=MESH,
+        )
+
+    for h in range(HALVES):
+        for i in range(1, PLANE):
+            plane_reduce(h, i).start()
+
+    token_swap.wait_recv()
+    add_own(gt, gt_in, half_tok)
+    token_out = pltpu.make_async_copy(gt_in, gt_hbm, out_sem.at[0])
+    token_out.start()
+
+    for h in range(HALVES):
+        for i in range(1, PLANE):
+            plane_reduce(h, i).wait_recv()
+        acc = kt[chunk(h, my_q)].astype(F32)
+        for i in range(1, PLANE):
+            acc = acc + p1_in[h, i - 1].astype(F32)
+        p1_sum[h] = acc.astype(BF)
+        for i in range(1, depth):
+            column_reduce(h, i).start()
+
+    wait_recv_all(*gvs)
+    gather_sum(gv_in, pv)
+
+    def store_grad(i, carry):
+        rows = pl.ds(pl.multiple_of(i * TILE, TILE), TILE)
+        gs[:, rows] = (nt(pk[...], wk[rows, :]) + nt(pv[...], wv[rows, :])).astype(BF)
+        return carry
+
+    lax.fori_loop(0, width // TILE, store_grad, 0)
+    store_swap = to_partner(gs, gs_in, half_store, 1)
+    store_swap.start()
+
+    for h in range(HALVES):
+        for i in range(1, depth):
+            column_reduce(h, i).wait_recv()
+        acc = p1_sum[h, my_z].astype(F32)
+        for i in range(1, depth):
+            acc = acc + p2_in[h, i - 1].astype(F32)
+        kg[(h * PLANE + my_q) * depth + my_z] = acc.astype(BF)
+        for i in range(1, depth):
+            column_gather(h, i, my_z).start()
+
+    store_swap.wait_recv()
+    add_own(gs, gs_in, half_store)
+    store_out = pltpu.make_async_copy(gs_in, gs_hbm, out_sem.at[1])
+    store_out.start()
+
+    for h in range(HALVES):
+        for i in range(1, depth):
+            column_gather(h, i, lax.rem(my_z + depth - i, depth)).wait_recv()
+        for i in range(1, PLANE):
+            plane_gather(h, i, my_q).start()
+    for h in range(HALVES):
+        for i in range(1, PLANE):
+            plane_gather(h, i, lax.rem(my_q + PLANE - i, PLANE)).wait_recv()
+    weight_out = pltpu.make_async_copy(kg, gkw_hbm, out_sem.at[2])
+    weight_out.start()
+
+    wait_send_all(*reqs)
+    wait_send_all(*kvs)
+    wait_send_all(*gks)
+    wait_send_all(*gvs)
+    token_swap.wait_send()
+    store_swap.wait_send()
+    for h in range(HALVES):
+        for i in range(1, PLANE):
+            plane_reduce(h, i).wait_send()
+            plane_gather(h, i, my_q).wait_send()
+        for i in range(1, depth):
+            column_reduce(h, i).wait_send()
+            column_gather(h, i, my_z).wait_send()
+    token_out.wait()
+    store_out.wait()
+    weight_out.wait()
+
+
+def per_device(sizes, *args):
+    (tokens, store, ids, wq, wk, wv, wrq, wrk, wrv, rate, gain, gate, og) = args
+    n = sizes["st"]
+    pass_dev, plen, width = store.shape
+    length = tokens.shape[0]
+    rows = pass_dev * plen
+    weight_cols = sum(w.shape[1] for w in (wq, wk, wv, wrq, wrk, wrv))
+    fits = (
+        sizes["tp"] == 2
+        and wk.shape[1] == HEAD
+        and ids.size == n
+        and n % PLANE == 0
+        and width % (HALVES * n) == 0
+        and TILE % (width // (HALVES * n)) == 0
+        and width * weight_cols + n * plen * HEAD * 12 + length * width * 12 < 24 * 2**20
+    )
+    if not fits:
+        return per_device_plain(*args)
+    depth = n // PLANE
+    piece = width // (HALVES * n)
+
+    def vm(*shape, dtype=BF):
+        return pltpu.VMEM(shape, dtype)
+
+    any_spec = pl.BlockSpec(memory_space=pl.ANY)
+    smem = pl.BlockSpec(memory_space=pltpu.SMEM)
+    vmem = pl.BlockSpec(memory_space=pltpu.VMEM)
+    dma = pltpu.SemaphoreType.DMA
+    like = [vm(*x.shape) for x in (tokens,)] + [vm(rows, width)]
+    like += [vm(*x.shape) for x in (wq, wk, wv, wrq, wrk, wrv, og)]
+    qs = [vm(length, w.shape[1]) for w in (wq, wrq, wrk, wrv)]
+    scratch = (
+        like
+        + qs
+        + qs
+        + [
+            vm(length, width, dtype=F32),
+            vm(length, width),
+            vm(length // 2, width),
+            vm(rows, width),
+            vm(rows // 2, width),
+            vm(rows, 2 * HEAD),
+            vm(n, 8, 128, dtype=jnp.int32),
+            vm(n, 8, 128, dtype=jnp.int32),
+            vm(n, plen, 2 * HEAD),
+            vm(n, plen, 2 * HEAD),
+        ]
+        + [vm(n, plen, HEAD)] * 6
+        + [
+            vm(rows, HEAD),
+            vm(rows, HEAD),
+            vm(HALVES * n, piece, HEAD),
+            vm(HALVES, PLANE - 1, depth, piece, HEAD),
+            vm(HALVES, depth, piece, HEAD),
+            vm(HALVES, depth - 1, piece, HEAD),
+            vm(HALVES * n, piece, HEAD),
+            pltpu.SMEM((n,), jnp.int32),
+            pltpu.SMEM((n,), jnp.int32),
+            dma((9,)),
+            dma((3,)),
+            dma((2,)),
+            dma((2,)),
+        ]
+        + [dma((n,))] * 8
+        + [dma((HALVES, PLANE - 1))] * 2
+        + [dma((HALVES, depth - 1))] * 4
+        + [dma((HALVES, PLANE - 1))] * 2
+    )
+    grad_tokens, grad_store, grad_key = pl.pallas_call(
+        functools.partial(fused_kernel, n),
+        out_shape=(
+            jax.ShapeDtypeStruct((length // 2, width), BF),
+            jax.ShapeDtypeStruct((rows // 2, width), BF),
+            jax.ShapeDtypeStruct((HALVES * n, piece, HEAD), BF),
+        ),
+        in_specs=[smem, smem, vmem, vmem] + [any_spec] * 9,
+        out_specs=(any_spec, any_spec, any_spec),
+        scratch_shapes=scratch,
+        compiler_params=pltpu.CompilerParams(
+            collective_id=0, has_side_effects=True, vmem_limit_bytes=60 * 2**20
+        ),
+    )(
+        ids,
+        rate,
+        gain.reshape(1, -1),
+        gate.reshape(1, -1),
+        tokens,
+        store.reshape(rows, width),
+        wq,
+        wk,
+        wv,
+        wrq,
+        wrk,
+        wrv,
+        og,
+    )
+    return (
+        grad_tokens,
+        grad_store.reshape(pass_dev // 2, plen, width),
+        grad_key.reshape(width, HEAD).astype(F32),
+    )
+
+
 def solution(mesh):
     return jax.shard_map(
-        per_device,
+        functools.partial(per_device, dict(mesh.shape)),
         mesh=mesh,
         in_specs=(
             P("st", None),

time: 244 us -> 98.4 us (0.40)
  waiting for transfers between devices: 131 us -> 0 us
  Pallas kernels: 0 us -> 93.1 us
  matrix products: 40.1 us -> 0 us
  local copies, waits for them, and re-layouts: 31.6 us -> 1.59 us
  starting transfers between devices: 19 us -> 0 us
  between operations: 16 us -> 0.66 us
  other arithmetic: 5.71 us -> 2.79 us
    psum x1 -> x0, waiting for transfers between devices: 113 us -> none  [per_device(): grad_key_weight = lax.psum(key_term, 'st')]
    pallas_call x0 -> x1, Pallas kernels: none -> 93.1 us  [per_device(): pl.pallas_call(functools.partial(fused_kernel, n), out_shape=(jax.ShapeDt...]
    dot_general x29 -> x0, matrix products: 40.1 us -> none  [the longest x6 10.7 us: against_rows(): lax.dot_general(left, weight, (((1,), (1,)), ((), ())), preferred_element...]
    all_to_all x3 -> x0, starting transfers between devices: 18.6 us -> none  [the longest x1 8.34 us: per_device(): lax.all_to_all(request, 'st', split_axis=0, concat_axis=0, tiled=True)]
    all_to_all x3 -> x0, waiting for transfers between devices: 17.9 us -> none  [the longest x1 13.5 us: per_device(): lax.all_to_all(outgoing, 'st', split_axis=0, concat_axis=0, tiled=True)]
    unnamed x61 -> x6, local copies, waits for them, and re-layouts: 13.2 us -> 1.59 us
    reshape x6 -> x0, local copies, waits for them, and re-layouts: 10 us -> none  [the longest x2 4.98 us: per_device(): out_grad.astype(jnp.float32).reshape(blocks, BLK, kv_local, group, HEAD)]
    convert_element_type x2 -> x0, local copies, waits for them, and re-layouts: 2.64 us -> none  [the longest x1 2.23 us: per_device(): out_grad.astype(jnp.float32).reshape(blocks, BLK, kv_local, group, HEAD)]
  transfers between devices with their start and end apart: 6 -> 0, of which waited for: 4 -> 0; matrix products, arithmetic and copies ran while one was open for 21% -> 0% of each run, Pallas kernels for 0% -> 0%
where the time goes in v1:
time: 98.4 us; the launch traced here: 98.2 us
  Pallas kernels  93.1 us (95%)
  other arithmetic  2.79 us (3%)
  local copies, waits for them, and re-layouts  1.59 us (2%)
    pallas_call x1, Pallas kernels, per_device(): pl.pallas_call(functools.partial(fused_kernel, n), out_shape=(jax.ShapeDt...  93.1 us
    convert_element_type x1, other arithmetic, per_device(): grad_key.reshape(width, HEAD).astype(F32)  2.79 us

profile of v1, /device:TPU:0, one launch (start us, length us, event | category | flops | bytes accessed | tf_op | source)
XLA Modules:
  0.0 98.2 jit_solution(2211554540616629298)
XLA Ops:
  0.6 93.1 %shard_map.148 = (bf16[128,2048]{1,0:T(8,128)(2,1)}, bf16[128,2048]{1,0:T(8,128)(2,1)}, bf16[32,64,256]{2,1,0:T(8,128)(2,1)}) custom-call(s32[4,4]{1,0:T(4,128)} %ids_ref.1, f32[4]{0:T(128)} %rate_ref.1, f32[1,1024]{1,0:T(1,128)} %bitcast.9, f32[1,1024]{1,0:T(1,128)} %bitcast.10, bf16[256,2048]{1,0:T(8,128)(2,1)} %tokens_hbm.1, bf16[256,2048]{1,0:T(8,128)(2,1)} %bitcast.7, ...), custom_call_target="tpu_custom_call" | custom-call | tf_op jit(solution)/shard_map/pallas_call | solution.py:789
  93.8 0.0 copy-start.1
  93.8 0.0 copy-start
  93.8 2.8 %bitcast_convert_fusion = f32[2048,256]{1,0:T(8,128)} fusion(bf16[32,64,256]{2,1,0:T(8,128)(2,1)} %get-tuple-element.8), kind=kLoop, calls=%fused_computation | loop fusion | flops 524288 | bytes 3145728 | tf_op jit(solution)/shard_map/convert_element_type | solution.py:820
  96.6 0.0 copy-done.1
  96.6 0.8 copy.18
  97.4 0.0 copy-done
  97.4 0.8 copy.19
Async XLA Ops:
  93.8 2.8 %copy-start.1 = (bf16[128,2048]{1,0:T(8,128)(2,1)S(1)}, bf16[128,2048]{1,0:T(8,128)(2,1)}, u32[]{:S(2)}) copy-start(bf16[128,2048]{1,0:T(8,128)(2,1)} %get-tuple-element.12) | copy-start | bytes 1572868
  93.8 3.6 %copy-start = (bf16[128,2048]{1,0:T(8,128)(2,1)S(1)}, bf16[128,2048]{1,0:T(8,128)(2,1)}, u32[]{:S(2)}) copy-start(bf16[128,2048]{1,0:T(8,128)(2,1)} %get-tuple-element.7) | copy-start | bytes 1572868

commit v2 on v1

--- a/solution.py
+++ b/solution.py
@@ -288,8 +288,8 @@
     gv_in,
     pk,
     pv,
-    kt,
-    p1_in,
+    slices,
+    pk_in,
     p1_sum,
     p2_in,
     kg,
@@ -309,6 +309,8 @@
     gv_recv,
     p1_send,
     p1_recv,
+    pk_send,
+    pk_recv,
     p2_send,
     p2_recv,
     p3_send,
@@ -448,6 +450,26 @@
     kv_in[me] = kv_out[me]
     start_all(*kvs)
 
+    span = slices.shape[3]
+
+    def columns_of(h, quarter):
+        return pl.ds(pl.multiple_of((h * PLANE + quarter) * span, span), span)
+
+    def share_rows(h, i):
+        other = lax.rem(my_q + i, PLANE)
+        return pltpu.make_async_remote_copy(
+            src_ref=store.at[:, columns_of(h, other)],
+            dst_ref=slices.at[h, i - 1],
+            send_sem=p1_send.at[h, i - 1],
+            recv_sem=p1_recv.at[h, i - 1],
+            device_id={"st": my_z * PLANE + other},
+            device_id_type=MESH,
+        )
+
+    for h in range(HALVES):
+        for i in range(1, PLANE):
+            share_rows(h, i).start()
+
     def project(w, out):
         def body(i, carry):
             cols = pl.ds(pl.multiple_of(i * TILE, TILE), TILE)
@@ -585,28 +607,16 @@
 
     wait_recv_all(*gks)
     gather_sum(gk_in, pk)
-    piece = kt.shape[1]
-    per_tile = TILE // piece
-
-    def key_term(i, carry):
-        cols = pl.ds(pl.multiple_of(i * TILE, TILE), TILE)
-        term = tn(store[:, cols], pk[...]).astype(BF)
-        kt[pl.ds(i * per_tile, per_tile)] = term.reshape(per_tile, piece, HEAD)
-        return carry
-
-    lax.fori_loop(0, width // TILE, key_term, 0)
-
     def chunk(h, quarter):
         return pl.ds((h * PLANE + quarter) * depth, depth)
 
-    def plane_reduce(h, i):
-        other = lax.rem(my_q + i, PLANE)
+    def share_key(i):
         return pltpu.make_async_remote_copy(
-            src_ref=kt.at[chunk(h, other)],
-            dst_ref=p1_in.at[h, i - 1],
-            send_sem=p1_send.at[h, i - 1],
-            recv_sem=p1_recv.at[h, i - 1],
-            device_id={"st": my_z * PLANE + other},
+            src_ref=pk,
+            dst_ref=pk_in.at[i - 1],
+            send_sem=pk_send.at[i - 1],
+            recv_sem=pk_recv.at[i - 1],
+            device_id={"st": my_z * PLANE + lax.rem(my_q + i, PLANE)},
             device_id_type=MESH,
         )
 
@@ -643,21 +653,24 @@
             device_id_type=MESH,
         )
 
-    for h in range(HALVES):
-        for i in range(1, PLANE):
-            plane_reduce(h, i).start()
+    for i in range(1, PLANE):
+        share_key(i).start()
+    own_terms = [tn(store[:, columns_of(h, my_q)], pk[...]) for h in range(HALVES)]
 
     token_swap.wait_recv()
     add_own(gt, gt_in, half_tok)
     token_out = pltpu.make_async_copy(gt_in, gt_hbm, out_sem.at[0])
     token_out.start()
 
+    for i in range(1, PLANE):
+        share_key(i).wait_recv()
+        for h in range(HALVES):
+            share_rows(h, i).wait_recv()
     for h in range(HALVES):
+        acc = own_terms[h]
         for i in range(1, PLANE):
-            plane_reduce(h, i).wait_recv()
-        acc = kt[chunk(h, my_q)].astype(F32)
-        for i in range(1, PLANE):
-            acc = acc + p1_in[h, i - 1].astype(F32)
+            acc = acc + tn(slices[h, i - 1], pk_in[i - 1])
+        acc = acc.reshape(p1_sum.shape[1:])
         p1_sum[h] = acc.astype(BF)
         for i in range(1, depth):
             column_reduce(h, i).start()
@@ -708,11 +721,13 @@
     store_swap.wait_send()
     for h in range(HALVES):
         for i in range(1, PLANE):
-            plane_reduce(h, i).wait_send()
+            share_rows(h, i).wait_send()
             plane_gather(h, i, my_q).wait_send()
         for i in range(1, depth):
             column_reduce(h, i).wait_send()
             column_gather(h, i, my_z).wait_send()
+    for i in range(1, PLANE):
+        share_key(i).wait_send()
     token_out.wait()
     store_out.wait()
     weight_out.wait()
@@ -731,7 +746,8 @@
         and ids.size == n
         and n % PLANE == 0
         and width % (HALVES * n) == 0
-        and TILE % (width // (HALVES * n)) == 0
+        and width % (HALVES * PLANE * 128) == 0
+        and width // (HALVES * n) % 16 == 0
         and width * weight_cols + n * plen * HEAD * 12 + length * width * 12 < 24 * 2**20
     )
     if not fits:
@@ -769,8 +785,8 @@
         + [
             vm(rows, HEAD),
             vm(rows, HEAD),
-            vm(HALVES * n, piece, HEAD),
-            vm(HALVES, PLANE - 1, depth, piece, HEAD),
+            vm(HALVES, PLANE - 1, rows, width // (HALVES * PLANE)),
+            vm(PLANE - 1, rows, HEAD),
             vm(HALVES, depth, piece, HEAD),
             vm(HALVES, depth - 1, piece, HEAD),
             vm(HALVES * n, piece, HEAD),
@@ -783,6 +799,7 @@
         ]
         + [dma((n,))] * 8
         + [dma((HALVES, PLANE - 1))] * 2
+        + [dma((PLANE - 1,))] * 2
         + [dma((HALVES, depth - 1))] * 4
         + [dma((HALVES, PLANE - 1))] * 2
     )

time: 98.4 us -> 91.9 us (0.934)
  Pallas kernels: 93.1 us -> 86.7 us
    pallas_call x1, Pallas kernels: 93.1 us -> 86.7 us  [per_device(): pl.pallas_call(functools.partial(fused_kernel, n), out_shape=(jax.ShapeDt...]
where the time goes in v2:
time: 91.9 us; the launch traced here: 91.7 us
  Pallas kernels  86.7 us (94%)
  other arithmetic  2.79 us (3%)
  local copies, waits for them, and re-layouts  1.59 us (2%)
    pallas_call x1, Pallas kernels, per_device(): pl.pallas_call(functools.partial(fused_kernel, n), out_shape=(jax.ShapeDt...  86.7 us
    convert_element_type x1, other arithmetic, per_device(): grad_key.reshape(width, HEAD).astype(F32)  2.79 us

profile of v2, /device:TPU:0, one launch (start us, length us, event | category | flops | bytes accessed | tf_op | source)
XLA Modules:
  0.0 91.7 jit_solution(15831450202814641108)
XLA Ops:
  0.6 86.7 %shard_map.148 = (bf16[128,2048]{1,0:T(8,128)(2,1)}, bf16[128,2048]{1,0:T(8,128)(2,1)}, bf16[32,64,256]{2,1,0:T(8,128)(2,1)}) custom-call(s32[4,4]{1,0:T(4,128)} %ids_ref.1, f32[4]{0:T(128)} %rate_ref.1, f32[1,1024]{1,0:T(1,128)} %bitcast.9, f32[1,1024]{1,0:T(1,128)} %bitcast.10, bf16[256,2048]{1,0:T(8,128)(2,1)} %tokens_hbm.1, bf16[256,2048]{1,0:T(8,128)(2,1)} %bitcast.7, ...), custom_call_target="tpu_custom_call" | custom-call | tf_op jit(solution)/shard_map/pallas_call | solution.py:806
  87.3 0.0 copy-start.1
  87.3 0.0 copy-start
  87.4 2.8 %bitcast_convert_fusion = f32[2048,256]{1,0:T(8,128)} fusion(bf16[32,64,256]{2,1,0:T(8,128)(2,1)} %get-tuple-element.8), kind=kLoop, calls=%fused_computation | loop fusion | flops 524288 | bytes 3145728 | tf_op jit(solution)/shard_map/convert_element_type | solution.py:837
  90.1 0.0 copy-done.1
  90.1 0.8 copy.18
  90.9 0.0 copy-done
  90.9 0.8 copy.19
Async XLA Ops:
  87.3 2.8 %copy-start.1 = (bf16[128,2048]{1,0:T(8,128)(2,1)S(1)}, bf16[128,2048]{1,0:T(8,128)(2,1)}, u32[]{:S(2)}) copy-start(bf16[128,2048]{1,0:T(8,128)(2,1)} %get-tuple-element.12) | copy-start | bytes 1572868
  87.3 3.6 %copy-start = (bf16[128,2048]{1,0:T(8,128)(2,1)S(1)}, bf16[128,2048]{1,0:T(8,128)(2,1)}, u32[]{:S(2)}) copy-start(bf16[128,2048]{1,0:T(8,128)(2,1)} %get-tuple-element.7) | copy-start | bytes 1572868
